TPU v7x, 32 devices: a whole 2x2x4 slice. The times are simulated.
32 devices in a mesh: grp: 2 (over x), sp: 8 (over z, y), tp: 2 (over core).
Axes of the slice: x: 2, y: 2, z: 4, core: 2. Of those that a mesh axis runs over, the one named last changes fastest.
Arguments:
- gate_in: bfloat16 [6144, 2048], P(('grp', 'sp'), 'tp'), parts along dimension 0, may hold values from -6 to 6
- values_in: bfloat16 [6144, 2048], P(('grp', 'sp'), 'tp'), parts along dimension 0, may hold values from -6 to 6
- input_state_in: bfloat16 [6144, 512], P(('grp', 'sp'), 'tp'), parts along dimension 0, may hold values from -6 to 6
- output_state_in: bfloat16 [6144, 512], P(('grp', 'sp'), 'tp'), parts along dimension 0, may hold values from -6 to 6
- step_in: bfloat16 [6144, 32], P(('grp', 'sp'), 'tp'), parts along dimension 0, may hold values from -6 to 6
- conv_x: bfloat16 [4, 2048], P(None, 'tp'), may hold values from -3 to 3
- conv_b: bfloat16 [4, 512], P(None, 'tp'), may hold values from -3 to 3
- conv_c: bfloat16 [4, 512], P(None, 'tp'), may hold values from -3 to 3
- dt_bias: float32 [32], P('tp'), may hold values from -1 to 1
- decay_rate: float32 [32], P('tp'), may hold values from 0 to 1, as said below
- log_decay_extra: float32 [6144, 32], P(('grp', 'sp'), 'tp'), parts along dimension 0, may hold values from -1 to 0
- out_gain: bfloat16 [2048], P('tp'), may hold values from 0.099609375 to 1.8984375
- w_out: bfloat16 [2048, 2048], P('tp'), may hold values from -0.125 to 0.125
Outputs:
- mixed: bfloat16 [6144, 2048], P(('grp', 'sp', 'tp')), parts along dimension 0
There are 2 independent parts, one for each index of `grp`. A program takes and returns all parts, laid end to end along the dimension named above; an argument that names none is the same for every part. Nothing has to cross between parts.
Inputs may be any that keep to these rules, and one draw needn't show every extreme that they name: `decay_rate`: positive rates.
All inputs are finite; a program needn't handle non-finite values.
Results may differ from a plain program's by a relative error of at most 0.01.
Values may be sent and summed in bfloat16 or wider, within the bound.
A program may use at most 128 MiB of HBM per device.

v0:
```python
import jax
import jax.numpy as jnp
from jax import lax
from jax.sharding import PartitionSpec as P

HEAD_DIM = 64
STATE = 128
CONV = 4
BLOCK = 128


def shifted(block, axis, distance):
    devices = range(lax.axis_size(axis))
    route = [(i - distance, i) for i in devices if i - distance in devices]
    return lax.ppermute(block, axis, route)


def prefix_2(part, axis, combine, identity):
    place = lax.axis_index(axis)
    gathered = jax.tree.map(lambda a: lax.all_gather(a, axis), part)
    state = jax.tree.map(lambda a, e: jnp.zeros_like(a) + jnp.asarray(e, a.dtype), part, identity)

    def one(turn, state):
        return combine(
            state, jax.tree.map(lambda a: lax.dynamic_index_in_dim(a, turn, 0, False), gathered)
        )

    return lax.fori_loop(0, place, one, state)


def rms_rows(values, gain, epsilon):
    scaled = values * lax.rsqrt(jnp.mean(values * values, axis=-1, keepdims=True) + epsilon)
    return scaled * gain.astype(jnp.float32)


def run_chain(initial, decays, parts):

    def advance(state, inputs):
        factor, part_state = inputs
        return (state * factor[:, None, None] + part_state, state)

    return lax.scan(advance, initial, (decays, parts))


def combine_carry(earlier, later):
    return (earlier[0] * later[0], earlier[1] * later[0][:, None, None] + later[1])


def read_state(c_heads, states, cum_log):
    product = jnp.einsum(
        "cihn,chpn->cihp",
        c_heads,
        states,
        precision=lax.Precision.HIGHEST,
        preferred_element_type=jnp.float32,
    )
    return product * jnp.exp(cum_log)[..., None]


def body(
    gate_in,
    values_in,
    input_state_in,
    output_state_in,
    step_in,
    conv_x,
    conv_b,
    conv_c,
    dt_bias,
    decay_rate,
    log_decay_extra,
    out_gain,
    w_out,
):
    inner = values_in.shape[1]
    shared = input_state_in.shape[1]
    heads_local = step_in.shape[1]
    span = values_in.shape[0]
    conv_input = jnp.concatenate([values_in, input_state_in, output_state_in], axis=1)
    previous = shifted(conv_input[span - (CONV - 1) :], "sp", 1)
    extended = jnp.concatenate([previous, conv_input], axis=0)
    kernel = jnp.concatenate([conv_x, conv_b, conv_c], axis=1)
    summed = jnp.zeros(conv_input.shape, jnp.float32)
    for offset in range(CONV):
        summed = summed + kernel[offset].astype(jnp.float32) * extended[
            offset : offset + span
        ].astype(jnp.float32)
    activated = jax.nn.silu(summed).astype(jnp.bfloat16)
    x_input = activated[:, :inner]
    b_input = activated[:, inner : inner + shared]
    c_input = activated[:, inner + shared :]
    step_size = jax.nn.softplus(step_in.astype(jnp.float32) + dt_bias)
    log_step = log_decay_extra - step_size * decay_rate
    groups_local = shared // STATE
    per_group = heads_local // groups_local
    count = span // BLOCK
    x_blocks = x_input.reshape(count, BLOCK, heads_local, HEAD_DIM)
    b_blocks = b_input.reshape(count, BLOCK, groups_local, STATE)
    c_blocks = c_input.reshape(count, BLOCK, groups_local, STATE)
    cum_log = jnp.cumsum(log_step.reshape(count, BLOCK, heads_local), axis=1)
    cum_rows = jnp.swapaxes(cum_log, 1, 2)
    step_rows = jnp.swapaxes(step_size.reshape(count, BLOCK, heads_local), 1, 2)
    scores = jnp.einsum("cign,cjgn->cgij", c_blocks, b_blocks, preferred_element_type=jnp.float32)
    head_scores = jnp.repeat(scores, per_group, axis=1)
    lower = jnp.tril(jnp.ones((BLOCK, BLOCK), dtype=bool))
    decay = jnp.exp(jnp.where(lower, cum_rows[..., :, None] - cum_rows[..., None, :], -jnp.inf))
    mixing = (head_scores * decay * step_rows[:, :, None, :]).astype(jnp.bfloat16)
    y_diag = jnp.einsum("chij,cjhp->cihp", mixing, x_blocks, preferred_element_type=jnp.float32)
    to_end = jnp.exp(cum_rows[..., -1:] - cum_rows) * step_rows
    b_heads = (
        jnp.repeat(b_blocks, per_group, axis=2) * jnp.swapaxes(to_end, 1, 2)[..., None]
    ).astype(jnp.bfloat16)
    added = jnp.einsum("cjhp,cjhn->chpn", x_blocks, b_heads, preferred_element_type=jnp.float32)
    log_totals = cum_rows[..., -1]
    block_decay = jnp.exp(log_totals)
    c_heads = jnp.repeat(c_blocks, per_group, axis=2).astype(jnp.float32)
    zero_state = jnp.zeros((heads_local, HEAD_DIM, STATE), jnp.float32)
    final_local, entering_local = run_chain(zero_state, block_decay, added)
    device_decay = jnp.exp(jnp.sum(log_totals, axis=0))
    identity = (jnp.ones((heads_local,), jnp.float32), zero_state)
    _, carried = prefix_2((device_decay, final_local), "sp", combine_carry, identity)
    prefix = jnp.cumsum(log_totals, axis=0) - log_totals
    from_carry = jnp.einsum(
        "cihn,hpn->cihp",
        c_heads,
        carried,
        precision=lax.Precision.HIGHEST,
        preferred_element_type=jnp.float32,
    )
    y_state = (
        read_state(c_heads, entering_local, cum_log)
        + from_carry * jnp.exp(cum_log + prefix[:, None, :])[..., None]
    )
    mixed_heads = (y_diag + y_state).reshape(span, heads_local, HEAD_DIM)
    gated = mixed_heads * jax.nn.silu(gate_in.astype(jnp.float32)).reshape(
        span, heads_local, HEAD_DIM
    )
    normalized = (
        rms_rows(gated, out_gain.reshape(heads_local, HEAD_DIM), 1e-05)
        .astype(jnp.bfloat16)
        .reshape(span, inner)
    )
    token_rows = lax.all_to_all(normalized, "tp", split_axis=0, concat_axis=1, tiled=True)
    result = jnp.dot(
        token_rows,
        lax.all_gather(w_out, "tp", axis=0, tiled=True),
        preferred_element_type=jnp.float32,
    )
    return result.astype(jnp.bfloat16)


def solution(mesh):
    placed = (
        P(("grp", "sp"), "tp"),
        P(("grp", "sp"), "tp"),
        P(("grp", "sp"), "tp"),
        P(("grp", "sp"), "tp"),
        P(("grp", "sp"), "tp"),
        P(None, "tp"),
        P(None, "tp"),
        P(None, "tp"),
        P("tp"),
        P("tp"),
        P(("grp", "sp"), "tp"),
        P("tp"),
        P("tp", None),
    )
    return jax.shard_map(
        body, mesh=mesh, in_specs=placed, out_specs=P(("grp", "sp", "tp"), None), check_vma=False
    )
```

profile of v0, /device:TPU:28, one launch (start us, length us, event | category | flops | bytes accessed | tf_op | source)
XLA Modules:
  0.0 133.5 jit_solution(9978120094064109055)
XLA Ops:
  6.6 1.3 constant_dynamic-update-slice_fusion.5
  8.0 1.3 collective-permute-start
  9.4 0.1 compare_select_fusion
  9.5 0.1 copy.87
  9.6 0.2 reduce_window_sum.22
  9.9 0.1 copy.72
  10.0 0.8 fusion.34
  10.9 0.1 fusion.28
  11.0 0.1 copy.76
  11.1 2.5 %collective-permute-done = bf16[3,1536]{1,0:T(4,128)(2,1)S(1)} collective-permute-done((bf16[3,1536]{1,0:T(4,128)(2,1)S(1)}, bf16[3,1536]{1,0:T(4,128)(2,1)S(1)}, u32[]{:S(2)}, u32[]{:S(2)}) %collective-permute-start) | collective-permute-done | bytes 9248 | tf_op jit(solution)/shard_map/ppermute | solution.py:15
  13.6 1.6 %multiply_convert_fusion.2 = bf16[384,1536]{1,0:T(8,128)(2,1)S(1)} fusion(bf16[384,1536]{1,0:T(8,128)(2,1)S(1)} %constant_dynamic-update-slice_fusion.3, bf16[3,1536]{1,0:T(4,128)(2,1)S(1)} %collective-permute-done, f32[1536]{0:T(1024)S(1)} %get-tuple-element.99, f32[1536]{0:T(1024)S(1)} %get-tuple-element.100, f32[1536]{0:T(1024)S(1)} %get-tuple-element.101, ...), kind=kLoop, calls=%fused_computation.9 | loop fusion | flops 14745600 | bytes 2393088 | tf_op jit(solution)/shard_map/convert_element_type | solution.py:88
  15.2 0.7 fusion.33
  15.9 0.1 slice.58
  16.0 0.1 reshape.99
  16.1 0.8 copy.75
  16.9 1.0 reshape.118
  17.9 1.1 copy.74
  19.0 1.4 %broadcast_in_dim.32 = f32[3,128,2,8,128]{4,1,3,2,0:T(8,128)S(1)} broadcast(f32[3,128,2,128]{3,1,2,0:T(8,128)} %copy.75), dimensions={0,1,2,4} | broadcast | bytes 3538944 | tf_op jit(solution)/shard_map/broadcast_in_dim | solution.py:111
  20.4 1.6 %fusion.5 = f32[3,16,64,128]{3,2,1,0:T(8,128)S(1)} fusion(bf16[3,128,16,64]{1,3,2,0:T(8,128)(2,1)S(1)} %copy.74, f32[3,128,16,128]{3,1,2,0:T(8,128)S(1)} %bitcast.87, f32[3,128,16]{1,2,0:T(8,128)S(1)} %copy.76), kind=kOutput, calls=%fused_computation.18 | convolution fusion | flops 102236160 | bytes 5529600 | tf_op jit(solution)/shard_map/cjhp,cjhn->chpn/dot_general | solution.py:113
  22.0 3.0 %while.26 = (s32[]{:T(128)}, f32[16,64,128]{2,1,0:T(8,128)S(1)}, f32[3,16,64,128]{3,2,1,0:T(8,128)}, f32[3,16]{1,0:T(4,128)S(1)}, f32[3,16,64,128]{3,2,1,0:T(8,128)S(1)}, /*index=5*/s32[]{:T(128)}, s32[]{:T(128)}) while((s32[]{:T(128)}, f32[16,64,128]{2,1,0:T(8,128)S(1)}, f32[3,16,64,128]{3,2,1,0:T(8,128)}, f32[3,16]{1,0:T(4,128)S(1)}, ...), condition=%wide.region_2.3_spmd.clone, body=%wide.region_1.2_spmd.clone.sunk | while | flops 524291 | bytes 2622240 | solution.py:42
  22.0 0.8 bitcast_dynamic-update-slice_fusion.2
  22.9 0.1 bitcast_add_fusion.5
  23.0 0.8 bitcast_dynamic-update-slice_fusion.2
  23.8 0.1 bitcast_add_fusion.5
  24.0 0.8 bitcast_dynamic-update-slice_fusion.2
  24.8 0.1 bitcast_add_fusion.5
  25.0 0.8 copy-done
  25.9 0.7 all-gather.5.cloned.1.call-update
  26.6 0.1 copy.70
  26.7 0.7 dynamic-slice
  28.0 0.1 exponential_dynamic-update-slice_fusion
  28.1 17.2 %all-reduce = f32[128]{0:T(128)S(1)} all-reduce(f32[128]{0:T(128)S(1)} %exponential_dynamic-update-slice_fusion), channel_id=2, replica_groups=mesh['grp'=2,'sp'=8,'tp'=2] {'sp'}, use_global_device_ids=true, to_apply=%add | all-reduce | flops 128 | bytes 1024
  45.3 0.1 reshape.110
  45.4 0.1 copy.73
  45.5 0.1 copy.79
  45.6 0.1 copy.80
  45.7 0.4 copy.82
  46.1 0.4 convert_multiply_fusion
  46.5 1.7 %reshape.105 = f32[3,128,16,64]{1,0,3,2:T(4,128)} reshape(f32[384,1024]{0,1:T(8,128)S(1)} %convert_multiply_fusion) | data formatting | bytes 3145728 | tf_op jit(solution)/shard_map/reshape | solution.py:135
  48.2 1.0 reshape.98
  49.2 0.7 copy.67
  49.9 0.2 fusion.23
  50.1 0.4 broadcast_in_dim.26
  50.5 1.3 fusion.4
  51.8 45.6 %all-gather.7.cloned.1.call-done = f32[128,64,128]{2,1,0:T(8,128)} async-done(((f32[16,64,128]{2,1,0:T(8,128)}), f32[128,64,128]{2,1,0:T(8,128)}) %all-gather.7.cloned.1.call-update) | async-done | bytes 4194320 | tf_op jit(solution)/shard_map/all_gather | solution.py:20
  97.5 8.9 %while.25 = (s32[]{:T(128)}, f32[16,64,128]{2,1,0:T(8,128)S(1)}, s32[]{:T(128)}, f32[8,16]{1,0:T(8,128)S(1)}, f32[8,16,64,128]{3,2,1,0:T(8,128)}, /*index=5*/s32[]{:T(128)}, s32[]{:T(128)}, s32[]{:T(128)}) while((s32[]{:T(128)}, f32[16,64,128]{2,1,0:T(8,128)S(1)}, s32[]{:T(128)}, f32[8,16]{1,0:T(8,128)S(1)}, f32[8,16,64,128]{3,2,1,0:T(8,128)}, ...), condition=%wide.region_5.6_spmd, body=%wide.region_4.5_spmd.sunk | while | flops 262149 | bytes 1573183 | solution.py:28
  97.5 1.2 bitcast_add_fusion.4
  98.8 1.2 bitcast_add_fusion.4
  100.0 1.2 bitcast_add_fusion.4
  101.3 1.2 bitcast_add_fusion.4
  102.5 1.2 bitcast_add_fusion.4
  103.7 1.2 bitcast_add_fusion.4
  105.0 1.2 bitcast_add_fusion.4
  106.4 0.4 broadcast_in_dim.54
  106.8 2.2 %fusion.21 = f32[16,64,3,128]{3,1,0,2:T(8,128)S(1)} fusion(bf16[3,128,16,128]{3,1,2,0:T(8,128)(2,1)S(1)} %bitcast.84, f32[16,64,128]{2,1,0:T(8,128)S(1)} %get-tuple-element.79), kind=kOutput, calls=%fused_computation.39 | convolution fusion | flops 603979776 | bytes 3670016 | tf_op jit(solution)/shard_map/cihn,hpn->cihp/dot_general | solution.py:123
  109.0 0.4 copy-done.2
  109.4 3.2 %fusion.12 = (f32[3,128,16]{1,2,0:T(8,128)S(1)}, f32[3,128,16,64]{1,3,2,0:T(8,128)S(1)}) fusion(f32[3,128,16,64]{1,0,3,2:T(4,128)S(1)} %copy-done.1, f32[3,128,16]{1,2,0:T(8,128)S(1)} %copy.80, f32[16,64,3,128]{3,1,0,2:T(8,128)S(1)} %fusion.21, f32[3,128,16]{1,2,0:T(8,128)S(1)} %copy.79, f32[3,16,64,128]{3,2,1,0:T(8,128)S(1)} %copy-done.2, ...), kind=kOutput, calls=%fused_computation.29 | convolution fusion | flops 606726144 | bytes 9510912 | tf_op jit(solution)/shard_map/cihn,chpn->cihp/dot_general | solution.py:50
  112.6 1.1 copy.81
  113.7 0.6 fusion.8
  114.3 0.3 copy.85
  114.5 4.9 %all_to_all.19 = bf16[2,192,1024]{2,1,0:T(8,128)(2,1)S(1)} all-to-all(bf16[2,192,1024]{2,1,0:T(8,128)(2,1)S(1)} %bitcast.89), channel_id=1, replica_groups=mesh['grp'=2,'sp'=8,'tp'=2] {'tp'}, dimensions={0} | all-to-all | bytes 1572864 | tf_op jit(solution)/shard_map/all_to_all | solution.py:143
  119.5 0.1 copy.92
  119.6 1.1 all-gather.5.cloned.1.call-done
  120.6 6.1 %convolution_convert_fusion = bf16[192,2048]{1,0:T(8,128)(2,1)} fusion(bf16[192,2048]{1,0:T(8,128)(2,1)S(1)} %bitcast.96, bf16[2048,2048]{1,0:T(8,128)(2,1)} %all-gather.5.cloned.1.call-done), kind=kOutput, calls=%fused_computation.8 | convolution fusion | flops 1611005952 | bytes 9961472 | tf_op jit(solution)/shard_map/dot_general | solution.py:144
  (64 shorter events, 0.5 us)
Async XLA Ops:
  6.5 1.4 %copy-start.7 = (bf16[384,256]{1,0:T(8,128)(2,1)S(1)}, bf16[384,256]{1,0:T(8,128)(2,1)}, u32[]{:S(2)}) copy-start(bf16[384,256]{1,0:T(8,128)(2,1)} %param.19) | copy-start | bytes 589828
  6.5 1.4 %copy-start.8 = (bf16[384,256]{1,0:T(8,128)(2,1)S(1)}, bf16[384,256]{1,0:T(8,128)(2,1)}, u32[]{:S(2)}) copy-start(bf16[384,256]{1,0:T(8,128)(2,1)} %param.20) | copy-start | bytes 589828
  6.5 2.8 %copy-start.10 = (bf16[384,16]{0,1:T(8,128)(2,1)S(1)}, bf16[384,16]{0,1:T(8,128)(2,1)}, u32[]{:S(2)}) copy-start(bf16[384,16]{0,1:T(8,128)(2,1)} %param.21) | copy-start | bytes 36868
  6.5 2.8 %copy-start.15 = (f32[16]{0:T(128)S(1)}, f32[16]{0:T(128)}, u32[]{:S(2)}) copy-start(f32[16]{0:T(128)} %param.25) | copy-start | bytes 196
  6.5 2.8 %copy-start.16 = (f32[16]{0:T(128)S(1)}, f32[16]{0:T(128)}, u32[]{:S(2)}) copy-start(f32[16]{0:T(128)} %param.26) | copy-start | bytes 196
  6.5 2.8 %copy-start.9 = (f32[384,16]{0,1:T(8,128)S(1)}, f32[384,16]{0,1:T(8,128)}, u32[]{:S(2)}) copy-start(f32[384,16]{0,1:T(8,128)} %param.27) | copy-start | bytes 73732
  6.6 3.5 %copy-start.11 = (bf16[4,1024]{1,0:T(4,128)(2,1)S(1)}, bf16[4,1024]{1,0:T(4,128)(2,1)}, u32[]{:S(2)}) copy-start(bf16[4,1024]{1,0:T(4,128)(2,1)} %param.22) | copy-start | bytes 24580
  6.6 90.9 %all-gather.7.cloned.1.call-start = ((), (), s32[]{:S(2)}) async-start(), calls=%async_computation.2 | async-start | bytes 4718592 | tf_op jit(solution)/shard_map/all_gather | solution.py:20
  7.9 3.0 %copy-start.13 = (bf16[4,256]{1,0:T(4,128)(2,1)S(1)}, bf16[4,256]{1,0:T(4,128)(2,1)}, u32[]{:S(2)}) copy-start(bf16[4,256]{1,0:T(4,128)(2,1)} %param.23) | copy-start | bytes 6148
  7.9 3.0 %copy-start.14 = (bf16[4,256]{1,0:T(4,128)(2,1)S(1)}, bf16[4,256]{1,0:T(4,128)(2,1)}, u32[]{:S(2)}) copy-start(bf16[4,256]{1,0:T(4,128)(2,1)} %param.24) | copy-start | bytes 6148
  8.0 5.6 %collective-permute-start = (bf16[3,1536]{1,0:T(4,128)(2,1)S(1)}, bf16[3,1536]{1,0:T(4,128)(2,1)S(1)}, u32[]{:S(2)}, u32[]{:S(2)}) collective-permute-start(bf16[3,1536]{1,0:T(4,128)(2,1)S(1)} %slice.50), channel_id=1, source_target_pairs={{0,2},{2,4},{4,6},{6,8},{8,10},{10,12},{12,14},{1,3},{3,5},{5,7},{... | collective-permute-start | bytes 27656 | tf_op jit(solution)/shard_map/ppermute | solution.py:15
  25.0 0.8 copy-start
  25.8 0.9 copy-start.17
  25.8 19.7 %copy-start.6 = (f32[3,128,16]{2,1,0:T(8,128)S(1)}, f32[3,128,16]{2,1,0:T(8,128)}, u32[]{:S(2)}) copy-start(f32[3,128,16]{2,1,0:T(8,128)} %get-tuple-element.124) | copy-start | bytes 73732
  25.8 19.8 %copy-start.5 = (f32[3,128,16]{2,1,0:T(8,128)S(1)}, f32[3,128,16]{2,1,0:T(8,128)}, u32[]{:S(2)}) copy-start(f32[3,128,16]{2,1,0:T(8,128)} %get-tuple-element.125) | copy-start | bytes 73732
  25.8 19.9 %copy-start.4 = (bf16[384,1024]{1,0:T(8,128)(2,1)S(1)}, bf16[384,1024]{1,0:T(8,128)(2,1)}, u32[]{:S(2)}) copy-start(bf16[384,1024]{1,0:T(8,128)(2,1)} %param.17) | copy-start | bytes 2359300
  25.8 94.8 %all-gather.5.cloned.1.call-start = ((), (), s32[]{:S(2)}) async-start(), calls=%async_computation.1 | async-start | bytes 12582912 | tf_op jit(solution)/shard_map/all_gather | solution.py:146
  46.5 1.7 %copy-start.12 = (bf16[1024]{0:T(1024)(128)(2,1)S(1)}, bf16[1024]{0:T(1024)(128)(2,1)}, u32[]{:S(2)}) copy-start(bf16[1024]{0:T(1024)(128)(2,1)} %param.28) | copy-start | bytes 6148
  97.5 8.9 %copy-start.3 = (bf16[3,128,2,128]{3,1,2,0:T(8,128)(2,1)S(1)}, bf16[3,128,2,128]{3,1,2,0:T(8,128)(2,1)}, u32[]{:S(2)}) copy-start(bf16[3,128,2,128]{3,1,2,0:T(8,128)(2,1)} %copy.67) | copy-start | bytes 589828
  106.8 2.2 %copy-start.1 = (f32[3,128,16,64]{1,0,3,2:T(4,128)S(1)}, f32[3,128,16,64]{1,0,3,2:T(4,128)}, u32[]{:S(2)}) copy-start(f32[3,128,16,64]{1,0,3,2:T(4,128)} %reshape.105) | copy-start | bytes 4718596
  106.8 2.6 %copy-start.2 = (f32[3,16,64,128]{3,2,1,0:T(8,128)S(1)}, f32[3,16,64,128]{3,2,1,0:T(8,128)}, u32[]{:S(2)}) copy-start(f32[3,16,64,128]{3,2,1,0:T(8,128)} %get-tuple-element.77) | copy-start | bytes 4718596
Sparse Core Ops, SparseCore 0:
  25.9 71.4 all-gather.6
  99.0 21.5 all-gather.4
where the time goes:
time: 135 us; the launch traced here: 134 us
  waiting for transfers between devices  49.9 us (37%)
  blocking collectives  22.1 us (16%)
  local copies, waits for them, and re-layouts  15.3 us (11%)
  other arithmetic  15.2 us (11%)
  between operations  14.6 us (11%)
  matrix products  14.5 us (11%)
  starting transfers between devices  1.37 us (1%)
    all_gather x1, waiting for transfers between devices, prefix_2(): gathered = jax.tree.map(lambda a: lax.all_gather(a, axis), part)  45.6 us
    unnamed x1, blocking collectives  17.2 us
    add x7, other arithmetic, combine_carry(): earlier[1] * later[0][:, None, None] + later[1]  8.37 us
    dot_general x1, matrix products, body(): jnp.dot(token_rows, lax.all_gather(w_out, 'tp', axis=0, tiled=True), pref...  6.06 us
    all_to_all x1, blocking collectives, body(): lax.all_to_all(normalized, 'tp', split_axis=0, concat_axis=1, tiled=True)  4.94 us
    unnamed x45, local copies, waits for them, and re-layouts  3.77 us
    dot_general x1, matrix products, read_state(): jnp.einsum('cihn,chpn->cihp', c_heads, states, precision=lax.Precision.HI...  3.16 us
  transfers between devices with their start and end apart: 3, of which 3 were waited for; matrix products, arithmetic and copies ran while one was open for 19% of the time, Pallas kernels for 0%

commit v1 on v0

v1 whole, which is shorter than its diff:
```python
import functools

import jax
import jax.numpy as jnp
from jax import lax
from jax.experimental import pallas as pl
from jax.experimental.pallas import tpu as pltpu
from jax.sharding import PartitionSpec as P

HEAD_DIM = 64
STATE = 128
CONV = 4
BLOCK = 128
HALO = 16
CHUNKS = 4
LANES = 128
WIDE = 256
MESH = pl.DeviceIdType.MESH
F32 = jnp.float32
BF16 = jnp.bfloat16


def silu(v):
    return v / (1.0 + jnp.exp(-v))


def split(v):
    high = v.astype(BF16)
    return high, (v - high.astype(F32)).astype(BF16)


def spread(v, table):
    high, low = split(v)
    return jnp.dot(high, table, preferred_element_type=F32) + jnp.dot(
        low, table, preferred_element_type=F32
    )


def kernel(
    n,
    gate_ref,
    values_ref,
    b_ref,
    c_ref,
    step_ref,
    kx_ref,
    kb_ref,
    kc_ref,
    bias_ref,
    rate_ref,
    extra_ref,
    gain_ref,
    w_ref,
    out_ref,
    stage,
    act,
    weight,
    table,
    to_end,
    growth,
    cum_scr,
    cum_t,
    added,
    y_diag,
    gate_act,
    grown,
    decays,
    message,
    pair_in,
    state_in,
    state_out,
    partner_out,
    carried,
    normed,
    part_out,
    part_in,
    load_sem,
    halo_send,
    halo_recv,
    m1_send,
    m1_recv,
    m2_send,
    m2_recv,
    m3_send,
    m3_recv,
    tp_send,
    tp_recv,
):
    sp = lax.axis_index("sp")
    tp = lax.axis_index("tp")
    place = sp % 2
    pair = sp // 2
    pairs = n // 2
    span, inner = gate_ref.shape
    shared = b_ref.shape[1]
    count = span // BLOCK
    heads = inner // HEAD_DIM
    half = inner // 2
    rows_out, width = out_ref.shape
    pieces = width // WIDE

    loads = [
        pltpu.make_async_copy(values_ref, stage.at[pl.ds(HALO, span), pl.ds(0, inner)], load_sem.at[0]),
        pltpu.make_async_copy(b_ref, stage.at[pl.ds(HALO, span), pl.ds(inner, shared)], load_sem.at[1]),
        pltpu.make_async_copy(
            c_ref, stage.at[pl.ds(HALO, span), pl.ds(inner + shared, shared)], load_sem.at[2]
        ),
        pltpu.make_async_copy(w_ref, weight, load_sem.at[3]),
    ]
    for load in loads:
        load.start()

    barrier = pltpu.get_barrier_semaphore()
    for distance in (1, 2):

        @pl.when(sp >= distance)
        def _():
            pl.semaphore_signal(barrier, inc=1, device_id={"sp": sp - distance}, device_id_type=MESH)

        @pl.when(sp + distance < n)
        def _():
            pl.semaphore_signal(barrier, inc=1, device_id={"sp": sp + distance}, device_id_type=MESH)

    pl.semaphore_signal(barrier, inc=1, device_id={"tp": 1 - tp}, device_id_type=MESH)
    peers = 1
    for distance in (1, 2):
        peers = peers + jnp.where(sp >= distance, 1, 0) + jnp.where(sp + distance < n, 1, 0)
    pl.semaphore_wait(barrier, peers)

    halos = []
    for i, (source, start, size) in enumerate(
        ((values_ref, 0, inner), (b_ref, inner, shared), (c_ref, inner + shared, shared))
    ):
        halos.append(
            pltpu.make_async_remote_copy(
                src_ref=source.at[pl.ds(span - HALO, HALO), :],
                dst_ref=stage.at[pl.ds(0, HALO), pl.ds(start, size)],
                send_sem=halo_send.at[i],
                recv_sem=halo_recv.at[i],
                device_id={"sp": jnp.minimum(sp + 1, n - 1)},
                device_id_type=MESH,
            )
        )

    @pl.when(sp + 1 < n)
    def _():
        for copy in halos:
            copy.start()

    @pl.when(sp == 0)
    def _():
        stage[pl.ds(0, HALO), :] = jnp.zeros((HALO, stage.shape[1]), BF16)

    head_of = lax.broadcasted_iota(jnp.int32, (heads, inner), 1) // HEAD_DIM
    row_of = lax.broadcasted_iota(jnp.int32, (heads, inner), 0)
    table[...] = jnp.where(head_of == row_of, 1.0, 0.0).astype(BF16)
    step = jax.nn.softplus(step_ref[...].astype(F32) + bias_ref[...])
    log_step = extra_ref[...] - step * rate_ref[...]
    ri = lax.broadcasted_iota(jnp.int32, (BLOCK, BLOCK), 0)
    ci = lax.broadcasted_iota(jnp.int32, (BLOCK, BLOCK), 1)
    lower = jnp.where(ri >= ci, 1.0, 0.0).astype(F32)
    totals = []
    for blk in range(count):
        rows = slice(blk * BLOCK, (blk + 1) * BLOCK)
        cum = jnp.dot(lower, log_step[rows], precision=lax.Precision.HIGHEST, preferred_element_type=F32)
        last = cum[BLOCK - 1 :, :]
        totals.append(jnp.exp(last))
        to_end[rows, :] = jnp.exp(last - cum) * step[rows]
        growth[rows, :] = jnp.exp(cum)
        cum_scr[rows, :] = cum
        wide = jnp.concatenate(
            [cum, step[rows], jnp.zeros((BLOCK, LANES - 2 * heads), F32)], axis=1
        )
        cum_t[blk] = wide.T[: 2 * heads, :]
    stacked = jnp.concatenate(totals + [jnp.zeros((8 - count, heads), F32)], axis=0)
    decays[...] = spread(stacked, table[...])

    def conv_tile(blk, taps_ref, column, offset):
        rows = pl.ds(pl.multiple_of(blk * BLOCK, BLOCK), BLOCK + HALO)
        window = stage[rows, pl.ds(pl.multiple_of(offset + column, LANES), LANES)].astype(F32)
        taps = taps_ref[:, pl.ds(column, LANES)].astype(F32)
        total = taps[CONV - 1 :, :] * window[HALO:]
        for j in range(CONV - 1):
            total = total + taps[j : j + 1, :] * pltpu.roll(window, CONV - 1 - j, axis=0)[HALO:]
        out_rows = pl.ds(pl.multiple_of(blk * BLOCK, BLOCK), BLOCK)
        act[out_rows, pl.ds(pl.multiple_of(offset + column, LANES), LANES)] = silu(total).astype(BF16)

    def early(blk):
        rows = pl.ds(pl.multiple_of(blk * BLOCK, BLOCK), BLOCK)
        for t in range(shared // LANES):
            conv_tile(blk, kb_ref, t * LANES, inner)
        for t in range(inner // LANES):
            conv_tile(blk, kx_ref, t * LANES, 0)
        ends_high, ends_low = split(to_end[rows, :])
        per = inner // (shared // STATE)
        for g in range(shared // STATE):
            b_blk = act[rows, pl.ds(inner + g * STATE, STATE)].astype(F32).T.astype(BF16)
            for t in range(per // WIDE):
                cols = pl.ds(g * per + t * WIDE, WIDE)
                scale = jnp.dot(ends_high, table[:, cols], preferred_element_type=F32) + jnp.dot(
                    ends_low, table[:, cols], preferred_element_type=F32
                )
                weighted = (act[rows, cols].astype(F32) * scale).astype(BF16)
                added[blk, :, cols] = jnp.dot(b_blk, weighted, preferred_element_type=F32)

    for i in range(3):
        loads[i].wait()

    @pl.loop(0, count - 1)
    def _(i):
        early(count - 1 - i)

    @pl.when(sp > 0)
    def _():
        for copy in halos:
            copy.wait_recv()

    @pl.loop(0, 1)
    def _(i):
        early(i)

    decay_all = decays[0:1, :]
    for blk in range(1, count):
        decay_all = decay_all * decays[blk : blk + 1, :]
    for s in range(2):
        piece = decay_all[:, s * half : (s + 1) * half]
        high, low = split(piece)
        message[s, 0:HALO, :] = jnp.concatenate(
            [high.astype(F32), low.astype(F32), jnp.zeros((HALO - 2, half), F32)], axis=0
        ).astype(BF16)
        for t in range(half // LANES):
            cols = pl.ds(s * half + t * LANES, LANES)
            for blk in range(1, count):
                added[blk, :, cols] = (
                    added[blk - 1, :, cols] * decays[blk : blk + 1, cols] + added[blk, :, cols]
                )
            message[s, HALO:, t * LANES : (t + 1) * LANES] = added[count - 1, :, cols].astype(BF16)

    partner = {"sp": pair * 2 + 1 - place}
    step_rows = STATE // CHUNKS
    first_copies, chain_copies, back_copies = [], [], []
    for i in range(CHUNKS):
        begin = 0 if i == 0 else HALO + i * step_rows
        size = HALO + step_rows if i == 0 else step_rows
        first_copies.append(
            pltpu.make_async_remote_copy(
                src_ref=message.at[1 - place, pl.ds(begin, size), :],
                dst_ref=pair_in.at[pl.ds(begin, size), :],
                send_sem=m1_send.at[i],
                recv_sem=m1_recv.at[i],
                device_id=partner,
                device_id_type=MESH,
            )
        )
        rows = pl.ds(i * step_rows, step_rows)
        chain_copies.append(
            pltpu.make_async_remote_copy(
                src_ref=state_out.at[rows, :],
                dst_ref=state_in.at[rows, :],
                send_sem=m2_send.at[i],
                recv_sem=m2_recv.at[i],
                device_id={"sp": jnp.where(sp + 2 < n, sp + 2, sp - 2)},
                device_id_type=MESH,
            )
        )
        back_copies.append(
            pltpu.make_async_remote_copy(
                src_ref=partner_out.at[rows, :],
                dst_ref=carried.at[place, rows, :],
                send_sem=m3_send.at[i],
                recv_sem=m3_recv.at[i],
                device_id=partner,
                device_id_type=MESH,
            )
        )
    for copy in first_copies:
        copy.start()

    per_group = heads // (shared // STATE)
    left = lax.broadcasted_iota(jnp.int32, (BLOCK, LANES), 1) < HEAD_DIM
    keep = ri >= ci

    @pl.loop(0, count)
    def _(blk):
        rows = pl.ds(pl.multiple_of(blk * BLOCK, BLOCK), BLOCK)
        for t in range(shared // LANES):
            conv_tile(blk, kc_ref, t * LANES, inner + shared)
        cum = cum_scr[rows, :]
        across = cum_t[blk]
        for g in range(shared // STATE):
            scores = lax.dot_general(
                act[rows, pl.ds(inner + shared + g * STATE, STATE)],
                act[rows, pl.ds(inner + g * STATE, STATE)],
                (((1,), (1,)), ((), ())),
                preferred_element_type=F32,
            )
            for h in range(g * per_group, (g + 1) * per_group, 2):
                mixes = []
                for k in (h, h + 1):
                    gap = jnp.where(keep, cum[:, k : k + 1] - across[k : k + 1, :], -jnp.inf)
                    mixes.append(
                        (scores * jnp.exp(gap) * across[heads + k : heads + k + 1, :]).astype(BF16)
                    )
                cols = pl.ds(h * HEAD_DIM, LANES)
                x_pair = act[rows, cols]
                zero = jnp.zeros_like(x_pair)
                stack = jnp.concatenate(
                    [jnp.where(left, x_pair, zero), jnp.where(left, zero, x_pair)], axis=0
                )
                y_diag[rows, cols] = jnp.dot(
                    jnp.concatenate(mixes, axis=1), stack, preferred_element_type=F32
                )
                gate_act[rows, cols] = silu(gate_ref[rows, cols].astype(F32))
        grown_high, grown_low = split(growth[rows, :])
        for t in range(inner // WIDE):
            cols = pl.ds(t * WIDE, WIDE)
            grown[rows, cols] = jnp.dot(
                grown_high, table[:, cols], preferred_element_type=F32
            ) + jnp.dot(grown_low, table[:, cols], preferred_element_type=F32)

    def decay_of(ref_rows):
        values = ref_rows.astype(F32)
        return values[0:1, :] + values[1:2, :]

    @pl.when(pair == 0)
    def _():
        state_in[...] = jnp.zeros_like(state_in)

    for i in range(CHUNKS):
        rows = pl.ds(i * step_rows, step_rows)
        from_rows = pl.ds(HALO + i * step_rows, step_rows)
        first_copies[i].wait_recv()
        if i == 0:
            own_decay = decay_of(message[place, 0:HALO, :])
            other_decay = decay_of(pair_in[0:HALO, :])
            decay_0 = jnp.where(place == 0, own_decay, other_decay)
            decay_1 = jnp.where(place == 0, other_decay, own_decay)
        own = message[place, from_rows, :].astype(F32)
        other = pair_in[from_rows, :].astype(F32)
        state_0 = jnp.where(place == 0, own, other)
        state_1 = jnp.where(place == 0, other, own)
        total = state_1 + decay_1 * state_0

        @pl.when(pair > 0)
        def _():
            chain_copies[i].wait_recv()

        entering = state_in[rows, :].astype(F32)

        @pl.when(pair + 1 < pairs)
        def _():
            state_out[rows, :] = (total + decay_1 * (decay_0 * entering)).astype(BF16)
            chain_copies[i].start()

        second = (state_0 + decay_0 * entering).astype(BF16)
        arrived = entering.astype(BF16)
        partner_out[rows, :] = jnp.where(place == 0, second, arrived)
        back_copies[i].start()
        carried[place, rows, :] = jnp.where(place == 0, arrived, second)

    for copy in back_copies:
        copy.wait_recv()
    loads[3].wait()

    wi = lax.broadcasted_iota(jnp.int32, (WIDE, WIDE), 0) // HEAD_DIM
    wj = lax.broadcasted_iota(jnp.int32, (WIDE, WIDE), 1) // HEAD_DIM
    same_head = jnp.where(wi == wj, 1.0, 0.0).astype(BF16)
    per = inner // (shared // STATE)
    for t in range(inner // WIDE):
        cols = pl.ds(t * WIDE, WIDE)
        s, offset = (t * WIDE) // half, (t * WIDE) % half
        g = (t * WIDE) // per
        state = carried[s, :, offset : offset + WIDE].astype(F32)
        gain = gain_ref[:, cols].astype(F32)
        for blk in range(count):
            rows = slice(blk * BLOCK, (blk + 1) * BLOCK)
            if blk == 0:
                entering = state
            else:
                prefix = decays[0:1, cols]
                for k in range(1, blk):
                    prefix = prefix * decays[k : k + 1, cols]
                entering = added[blk - 1, :, cols] + prefix * state
            read = jnp.dot(
                act[rows, pl.ds(inner + shared + g * STATE, STATE)],
                entering.astype(BF16),
                preferred_element_type=F32,
            )
            gated = (y_diag[rows, cols] + grown[rows, cols] * read) * gate_act[rows, cols]
            square = jnp.dot((gated * gated).astype(BF16), same_head, preferred_element_type=F32)
            normed[rows, cols] = (
                gated * lax.rsqrt(square * (1.0 / HEAD_DIM) + 1e-05) * gain
            ).astype(BF16)

    def tp_copy(i):
        return pltpu.make_async_remote_copy(
            src_ref=part_out.at[i],
            dst_ref=part_in.at[i],
            send_sem=tp_send.at[i],
            recv_sem=tp_recv.at[i],
            device_id={"tp": 1 - tp},
            device_id_type=MESH,
        )

    @pl.loop(0, pieces)
    def _(i):
        cols = pl.ds(pl.multiple_of(i * WIDE, WIDE), WIDE)
        there = pl.ds(pl.multiple_of((1 - tp) * rows_out, HALO), rows_out)
        part_out[i] = jnp.dot(
            normed[there, :], weight[:, cols], preferred_element_type=F32
        ).astype(BF16)
        tp_copy(i).start()

    @pl.loop(0, pieces)
    def _(i):
        cols = pl.ds(pl.multiple_of(i * WIDE, WIDE), WIDE)
        here = pl.ds(pl.multiple_of(tp * rows_out, HALO), rows_out)
        part = jnp.dot(normed[here, :], weight[:, cols], preferred_element_type=F32)
        tp_copy(i).wait_recv()
        out_ref[:, cols] = (part + part_in[i].astype(F32)).astype(BF16)

    @pl.loop(0, pieces)
    def _(i):
        tp_copy(i).wait_send()

    @pl.when(sp + 1 < n)
    def _():
        for copy in halos:
            copy.wait_send()

    @pl.when(pair + 1 < pairs)
    def _():
        for copy in chain_copies:
            copy.wait_send()

    for copy in first_copies + back_copies:
        copy.wait_send()


def body(
    n,
    gate_in,
    values_in,
    input_state_in,
    output_state_in,
    step_in,
    conv_x,
    conv_b,
    conv_c,
    dt_bias,
    decay_rate,
    log_decay_extra,
    out_gain,
    w_out,
):
    span, inner = gate_in.shape
    shared = input_state_in.shape[1]
    heads = step_in.shape[1]
    width = w_out.shape[1]
    half = inner // 2
    rows_out = span // 2
    count = span // BLOCK
    pieces = width // WIDE
    full = inner + 2 * shared
    vmem = pl.BlockSpec(memory_space=pltpu.VMEM)
    anywhere = pl.BlockSpec(memory_space=pl.ANY)
    dma = pltpu.SemaphoreType.DMA
    return pl.pallas_call(
        functools.partial(kernel, n),
        out_shape=jax.ShapeDtypeStruct((rows_out, width), BF16),
        in_specs=[vmem, anywhere, anywhere, anywhere] + [vmem] * 8 + [anywhere],
        out_specs=vmem,
        scratch_shapes=[
            pltpu.VMEM((HALO + span, full), BF16),
            pltpu.VMEM((span, full), BF16),
            pltpu.VMEM(w_out.shape, BF16),
            pltpu.VMEM((heads, inner), BF16),
            pltpu.VMEM((span, heads), F32),
            pltpu.VMEM((span, heads), F32),
            pltpu.VMEM((span, heads), F32),
            pltpu.VMEM((count, 2 * heads, BLOCK), F32),
            pltpu.VMEM((count, STATE, inner), F32),
            pltpu.VMEM((span, inner), F32),
            pltpu.VMEM((span, inner), F32),
            pltpu.VMEM((span, inner), F32),
            pltpu.VMEM((8, inner), F32),
            pltpu.VMEM((2, HALO + STATE, half), BF16),
            pltpu.VMEM((HALO + STATE, half), BF16),
            pltpu.VMEM((STATE, half), BF16),
            pltpu.VMEM((STATE, half), BF16),
            pltpu.VMEM((STATE, half), BF16),
            pltpu.VMEM((2, STATE, half), BF16),
            pltpu.VMEM((span, inner), BF16),
            pltpu.VMEM((pieces, rows_out, WIDE), BF16),
            pltpu.VMEM((pieces, rows_out, WIDE), BF16),
            dma((4,)),
            dma((3,)),
            dma((3,)),
            dma((CHUNKS,)),
            dma((CHUNKS,)),
            dma((CHUNKS,)),
            dma((CHUNKS,)),
            dma((CHUNKS,)),
            dma((CHUNKS,)),
            dma((pieces,)),
            dma((pieces,)),
        ],
        compiler_params=pltpu.CompilerParams(
            collective_id=0, has_side_effects=True, vmem_limit_bytes=56 * 1024 * 1024
        ),
    )(
        gate_in,
        values_in,
        input_state_in,
        output_state_in,
        step_in,
        conv_x,
        conv_b,
        conv_c,
        dt_bias.reshape(1, -1),
        decay_rate.reshape(1, -1),
        log_decay_extra,
        out_gain.reshape(1, -1),
        w_out,
    )


def solution(mesh):
    n = mesh.shape["sp"]
    placed = (
        P(("grp", "sp"), "tp"),
        P(("grp", "sp"), "tp"),
        P(("grp", "sp"), "tp"),
        P(("grp", "sp"), "tp"),
        P(("grp", "sp"), "tp"),
        P(None, "tp"),
        P(None, "tp"),
        P(None, "tp"),
        P("tp"),
        P("tp"),
        P(("grp", "sp"), "tp"),
        P("tp"),
        P("tp", None),
    )
    return jax.shard_map(
        functools.partial(body, n),
        mesh=mesh,
        in_specs=placed,
        out_specs=P(("grp", "sp", "tp"), None),
        check_vma=False,
    )
```

time: 135 us -> 35.8 us (0.27)
  waiting for transfers between devices: 49.9 us -> 0 us
  Pallas kernels: 0 us -> 29.1 us
  blocking collectives: 22.1 us -> 0 us
  other arithmetic: 15.2 us -> 0 us
  between operations: 14.6 us -> 0.01 us
  matrix products: 14.5 us -> 0 us
  local copies, waits for them, and re-layouts: 15.3 us -> 6.36 us
  starting transfers between devices: 1.37 us -> 0 us
    all_gather x2 -> x0, waiting for transfers between devices: 46.7 us -> none  [the longest x1 45.6 us: prefix_2(): gathered = jax.tree.map(lambda a: lax.all_gather(a, axis), part)]
    pallas_call x0 -> x1, Pallas kernels: none -> 29.1 us  [body(): pl.pallas_call(functools.partial(kernel, n), out_shape=jax.ShapeDtypeStru...]
    unnamed x1 -> x0, blocking collectives: 17.2 us -> none
    dot_general x6 -> x0, matrix products: 14.5 us -> none  [the longest x1 6.06 us: body(): jnp.dot(token_rows, lax.all_gather(w_out, 'tp', axis=0, tiled=True), pref...]
    add x10 -> x0, other arithmetic: 8.73 us -> none  [the longest x7 8.37 us: combine_carry(): earlier[1] * later[0][:, None, None] + later[1]]
    all_to_all x1 -> x0, blocking collectives: 4.94 us -> none  [body(): lax.all_to_all(normalized, 'tp', split_axis=0, concat_axis=1, tiled=True)]
    reshape x7 -> x1, local copies, waits for them, and re-layouts: 5.63 us -> 1.28 us  [body(): out_gain.reshape(1, -1)]
    dynamic_update_slice x3 -> x0, other arithmetic: 2.52 us -> none  [run_chain(): return lax.scan(advance, initial, (decays, parts))]
  transfers between devices with their start and end apart: 3 -> 0, of which waited for: 3 -> 0; matrix products, arithmetic and copies ran while one was open for 19% -> 0% of each run, Pallas kernels for 0% -> 0%
where the time goes in v1:
time: 35.8 us; the launch traced here: 35.5 us
  Pallas kernels  29.1 us (81%)
  local copies, waits for them, and re-layouts  6.36 us (18%)
    pallas_call x1, Pallas kernels, body(): pl.pallas_call(functools.partial(kernel, n), out_shape=jax.ShapeDtypeStru...  29.1 us
    unnamed x3, local copies, waits for them, and re-layouts  5.08 us
    reshape x1, local copies, waits for them, and re-layouts, body(): out_gain.reshape(1, -1)  1.28 us

profile of v1, /device:TPU:28, one launch (start us, length us, event | category | flops | bytes accessed | tf_op | source)
XLA Modules:
  0.0 35.5 jit_solution(5758663383697428257)
XLA Ops:
  0.0 1.3 %reshape.11.gain_ref = bf16[1,1024]{1,0:T(2,128)(2,1)} reshape(bf16[1024]{0:T(1024)(128)(2,1)} %param.24) | data formatting | bytes 4096 | tf_op jit(solution)/shard_map/reshape | solution.py:523
  1.3 1.4 %copy.14.step_ref = bf16[384,16]{1,0:T(8,128)(2,1)} copy(bf16[384,16]{0,1:T(8,128)(2,1)} %param.17) | data formatting | bytes 24576 | tf_op args[4]
  2.7 1.5 %copy.15.extra_ref = f32[384,16]{1,0:T(8,128)} copy(f32[384,16]{0,1:T(8,128)} %param.23) | data formatting | bytes 49152 | tf_op args[10]
  4.3 29.1 %shard_map.127 = bf16[192,2048]{1,0:T(8,128)(2,1)} custom-call(bf16[384,1024]{1,0:T(8,128)(2,1)} %gate_ref.1, bf16[384,1024]{1,0:T(8,128)(2,1)} %values_ref.1, bf16[384,256]{1,0:T(8,128)(2,1)} %b_ref.1, bf16[384,256]{1,0:T(8,128)(2,1)} %c_ref.1, bf16[384,16]{1,0:T(8,128)(2,1)} %copy.14.step_ref, bf16[4,1024]{1,0:T(4,128)(2,1)} %kx_ref.1, ...), custom_call_target="tpu_custom_call" | custom-call | tf_op jit(solution)/shard_map/pallas_call | solution.py:468
  33.4 2.1 %copy.17 = bf16[192,2048]{1,0:T(8,128)(2,1)} copy(bf16[192,2048]{1,0:T(8,128)(2,1)} %shard_map.127) | data formatting | bytes 1572864

commit v2 on v1

--- a/solution.py
+++ b/solution.py
@@ -38,7 +38,7 @@
 
 def kernel(
     n,
-    gate_ref,
+    gate_hbm,
     values_ref,
     b_ref,
     c_ref,
@@ -52,6 +52,7 @@
     gain_ref,
     w_ref,
     out_ref,
+    gate_ref,
     stage,
     act,
     weight,
@@ -91,7 +92,7 @@
     place = sp % 2
     pair = sp // 2
     pairs = n // 2
-    span, inner = gate_ref.shape
+    span, inner = gate_hbm.shape
     shared = b_ref.shape[1]
     count = span // BLOCK
     heads = inner // HEAD_DIM
@@ -106,6 +107,7 @@
             c_ref, stage.at[pl.ds(HALO, span), pl.ds(inner + shared, shared)], load_sem.at[2]
         ),
         pltpu.make_async_copy(w_ref, weight, load_sem.at[3]),
+        pltpu.make_async_copy(gate_hbm, gate_ref, load_sem.at[4]),
     ]
     for load in loads:
         load.start()
@@ -154,24 +156,32 @@
     head_of = lax.broadcasted_iota(jnp.int32, (heads, inner), 1) // HEAD_DIM
     row_of = lax.broadcasted_iota(jnp.int32, (heads, inner), 0)
     table[...] = jnp.where(head_of == row_of, 1.0, 0.0).astype(BF16)
-    step = jax.nn.softplus(step_ref[...].astype(F32) + bias_ref[...])
-    log_step = extra_ref[...] - step * rate_ref[...]
+    ei = lax.broadcasted_iota(jnp.int32, (heads, heads), 0)
+    ej = lax.broadcasted_iota(jnp.int32, (heads, heads), 1)
+    bias = jnp.sum(jnp.where(ei == ej, bias_ref[...], 0.0), axis=1, keepdims=True)
+    rate = jnp.sum(jnp.where(ei == ej, rate_ref[...], 0.0), axis=1, keepdims=True)
+    step = jax.nn.softplus(step_ref[...].astype(F32) + bias)
+    log_step = extra_ref[...] - step * rate
     ri = lax.broadcasted_iota(jnp.int32, (BLOCK, BLOCK), 0)
     ci = lax.broadcasted_iota(jnp.int32, (BLOCK, BLOCK), 1)
-    lower = jnp.where(ri >= ci, 1.0, 0.0).astype(F32)
+    upper = jnp.where(ri <= ci, 1.0, 0.0).astype(F32)
     totals = []
     for blk in range(count):
         rows = slice(blk * BLOCK, (blk + 1) * BLOCK)
-        cum = jnp.dot(lower, log_step[rows], precision=lax.Precision.HIGHEST, preferred_element_type=F32)
-        last = cum[BLOCK - 1 :, :]
-        totals.append(jnp.exp(last))
-        to_end[rows, :] = jnp.exp(last - cum) * step[rows]
-        growth[rows, :] = jnp.exp(cum)
-        cum_scr[rows, :] = cum
-        wide = jnp.concatenate(
-            [cum, step[rows], jnp.zeros((BLOCK, LANES - 2 * heads), F32)], axis=1
+        cum = jnp.dot(
+            log_step[:, rows], upper, precision=lax.Precision.HIGHEST, preferred_element_type=F32
         )
-        cum_t[blk] = wide.T[: 2 * heads, :]
+        last = cum[:, BLOCK - 1 :]
+        ends = jnp.exp(last - cum) * step[:, rows]
+        rise = jnp.exp(cum)
+        cum_t[blk] = jnp.concatenate([cum, step[:, rows]], axis=0)
+        turned = jnp.concatenate(
+            [cum, ends, rise, jnp.zeros((LANES - 3 * heads, BLOCK), F32)], axis=0
+        ).T
+        cum_scr[rows, :] = turned[:, :heads]
+        to_end[rows, :] = turned[:, heads : 2 * heads]
+        growth[rows, :] = turned[:, 2 * heads : 3 * heads]
+        totals.append(turned[BLOCK - 1 :, 2 * heads : 3 * heads])
     stacked = jnp.concatenate(totals + [jnp.zeros((8 - count, heads), F32)], axis=0)
     decays[...] = spread(stacked, table[...])
 
@@ -276,6 +286,7 @@
     for copy in first_copies:
         copy.start()
 
+    loads[4].wait()
     per_group = heads // (shared // STATE)
     left = lax.broadcasted_iota(jnp.int32, (BLOCK, LANES), 1) < HEAD_DIM
     keep = ri >= ci
@@ -371,7 +382,7 @@
         s, offset = (t * WIDE) // half, (t * WIDE) % half
         g = (t * WIDE) // per
         state = carried[s, :, offset : offset + WIDE].astype(F32)
-        gain = gain_ref[:, cols].astype(F32)
+        gain = gain_ref[cols].astype(F32).reshape(1, WIDE)
         for blk in range(count):
             rows = slice(blk * BLOCK, (blk + 1) * BLOCK)
             if blk == 0:
@@ -468,9 +479,10 @@
     return pl.pallas_call(
         functools.partial(kernel, n),
         out_shape=jax.ShapeDtypeStruct((rows_out, width), BF16),
-        in_specs=[vmem, anywhere, anywhere, anywhere] + [vmem] * 8 + [anywhere],
+        in_specs=[anywhere, anywhere, anywhere, anywhere] + [vmem] * 8 + [anywhere],
         out_specs=vmem,
         scratch_shapes=[
+            pltpu.VMEM((span, inner), BF16),
             pltpu.VMEM((HALO + span, full), BF16),
             pltpu.VMEM((span, full), BF16),
             pltpu.VMEM(w_out.shape, BF16),
@@ -493,7 +505,7 @@
             pltpu.VMEM((span, inner), BF16),
             pltpu.VMEM((pieces, rows_out, WIDE), BF16),
             pltpu.VMEM((pieces, rows_out, WIDE), BF16),
-            dma((4,)),
+            dma((5,)),
             dma((3,)),
             dma((3,)),
             dma((CHUNKS,)),
@@ -513,14 +525,14 @@
         values_in,
         input_state_in,
         output_state_in,
-        step_in,
+        step_in.T,
         conv_x,
         conv_b,
         conv_c,
         dt_bias.reshape(1, -1),
         decay_rate.reshape(1, -1),
-        log_decay_extra,
-        out_gain.reshape(1, -1),
+        log_decay_extra.T,
+        out_gain,
         w_out,
     )
 

time: 35.8 us -> 31.1 us (0.87)
  local copies, waits for them, and re-layouts: 6.36 us -> 2.09 us
    unnamed x3 -> x1, local copies, waits for them, and re-layouts: 5.08 us -> 2.09 us
    reshape x1 -> x0, local copies, waits for them, and re-layouts: 1.28 us -> none  [body(): out_gain.reshape(1, -1)]
where the time goes in v2:
time: 31.1 us; the launch traced here: 30.9 us
  Pallas kernels  28.8 us (93%)
  local copies, waits for them, and re-layouts  2.09 us (7%)
    pallas_call x1, Pallas kernels, body(): pl.pallas_call(functools.partial(kernel, n), out_shape=jax.ShapeDtypeStru...  28.8 us
    unnamed x1, local copies, waits for them, and re-layouts  2.09 us

profile of v2, /device:TPU:28, one launch (start us, length us, event | category | flops | bytes accessed | tf_op | source)
XLA Modules:
  0.0 30.9 jit_solution(2099721252215364261)
XLA Ops:
  0.0 28.8 %shard_map.127 = bf16[192,2048]{1,0:T(8,128)(2,1)} custom-call(bf16[384,1024]{1,0:T(8,128)(2,1)} %gate_hbm.1, bf16[384,1024]{1,0:T(8,128)(2,1)} %values_ref.1, bf16[384,256]{1,0:T(8,128)(2,1)} %b_ref.1, bf16[384,256]{1,0:T(8,128)(2,1)} %c_ref.1, bf16[16,384]{1,0:T(8,128)(2,1)} %bitcast.5, bf16[4,1024]{1,0:T(4,128)(2,1)} %kx_ref.1, bf16[4,256]{1,0:T(4,128)(2,1)} %kb_ref.1, ...), custom_call_target="tpu_custom_call" | custom-call | tf_op jit(solution)/shard_map/pallas_call | solution.py:479
  28.8 2.1 %copy.15 = bf16[192,2048]{1,0:T(8,128)(2,1)} copy(bf16[192,2048]{1,0:T(8,128)(2,1)} %shard_map.127) | data formatting | bytes 1572864
